TPU v7x, 32 devices: a whole 2x2x4 slice. The times are simulated.
32 devices in a mesh: fs: 4 (over y, x), tp: 8 (over z, core).
Axes of the slice: x: 2, y: 2, z: 4, core: 2. Of those that a mesh axis runs over, the one named last changes fastest.
Arguments:
- tokens: bfloat16 [4096, 2048], P(('fs', 'tp')), may hold values from -6 to 6
- up_weight: bfloat16 [2048, 4096], P('fs', 'tp'), may hold values from -0.125 to 0.125
- down_weight: bfloat16 [4096, 2048], P('tp', 'fs'), may hold values from -0.09375 to 0.09375
- cotangent: bfloat16 [4096, 2048], P(('fs', 'tp')), may hold values from -6 to 6
Outputs:
- input_grad: bfloat16 [4096, 2048], P(('fs', 'tp'))
- up_grad: float32 [2048, 4096], P('fs', 'tp')
- down_grad: float32 [4096, 2048], P('tp', 'fs')
All inputs are finite; a program needn't handle non-finite values.
Results may differ from a plain program's by a relative error of at most 0.018.
Values may be sent and summed in bfloat16 or wider, within the bound.
A program may use at most 128 MiB of HBM per device.

v0:
```python
import jax
import jax.numpy as jnp
from jax import lax
from jax.sharding import PartitionSpec as P


def shards(tokens, up_weight, down_weight, cotangent):
    rows_all, cot_all = (
        lax.all_gather(tokens, "tp", axis=0, tiled=True),
        lax.all_gather(cotangent, "tp", axis=0, tiled=True),
    )
    up_whole = lax.all_gather(up_weight, "fs", axis=0, tiled=True)
    pre = jnp.dot(rows_all, up_whole, preferred_element_type=jnp.float32)
    active = jnp.maximum(pre, 0.0)
    hidden = (active * active).astype(jnp.bfloat16)
    part = cot_all
    dhidden = lax.dot_general(
        part,
        lax.all_gather(down_weight, "fs", axis=1, tiled=True),
        (((1,), (1,)), ((), ())),
        preferred_element_type=jnp.float32,
    )
    dpre = (2.0 * active * dhidden).astype(jnp.bfloat16)
    count_all = tokens.shape[0] * lax.axis_size("fs") * lax.axis_size("tp")
    factor = 1.0 / jnp.sqrt(jnp.float32(count_all))
    part = rows_all
    up_grad = (
        lax.psum_scatter(
            lax.dot_general(
                part, dpre, (((0,), (0,)), ((), ())), preferred_element_type=jnp.float32
            ).astype(jnp.bfloat16),
            "fs",
            scatter_dimension=0,
            tiled=True,
        ).astype(jnp.float32)
        * factor
    )
    down_term = lax.dot_general(
        hidden, cot_all, (((0,), (0,)), ((), ())), preferred_element_type=jnp.float32
    )
    down_grad = (
        lax.psum_scatter(
            down_term.astype(jnp.bfloat16), "fs", scatter_dimension=1, tiled=True
        ).astype(jnp.float32)
        * factor
    )
    part = dpre
    prod = lax.dot_general(
        part, up_whole, (((1,), (1,)), ((), ())), preferred_element_type=jnp.float32
    )
    rounded = lax.optimization_barrier(prod.astype(jnp.bfloat16))
    grad_rows = lax.psum_scatter(
        rounded.astype(jnp.float32).astype(jnp.bfloat16), "tp", scatter_dimension=0, tiled=True
    )
    return (grad_rows, up_grad, down_grad)


def solution(mesh):
    placed = (P(("fs", "tp"), None), P("fs", "tp"), P("tp", "fs"), P(("fs", "tp"), None))
    return jax.shard_map(
        shards,
        mesh=mesh,
        in_specs=placed,
        out_specs=(P(("fs", "tp"), None), P("fs", "tp"), P("tp", "fs")),
        check_vma=False,
    )
```

profile of v0, /device:TPU:0, one launch (start us, length us, event | category | flops | bytes accessed | tf_op | source)
XLA Modules:
  0.0 314.8 jit_solution(16396900336464673650)
XLA Ops:
  7.2 0.0 all-gather.7.cloned.1.call-start
  7.2 0.7 all-gather.7.cloned.1.call-update
  7.9 0.0 all-gather.5.cloned.1.call-start
  7.9 0.7 all-gather.5.cloned.1.call-update
  8.6 0.0 all-gather.9.cloned.1.call-start
  8.7 0.7 all-gather.9.cloned.1.call-update
  9.4 0.0 all-gather.11.cloned.1.call-start
  9.4 0.5 all-gather.11.cloned.1.call-update
  10.0 0.0 reduce-scatter.8.cloned.1.call-start
  10.0 37.7 %all-gather.7.cloned.1.call-done = bf16[2048,512]{1,0:T(8,128)(2,1)} async-done(((bf16[512,512]{1,0:T(8,128)(2,1)}), bf16[2048,512]{1,0:T(8,128)(2,1)}) %all-gather.7.cloned.1.call-update) | async-done | bytes 2097168 | tf_op jit(solution)/shard_map/all_gather | solution.py:12
  47.8 48.5 %all-gather.5.cloned.1.call-done = bf16[1024,2048]{1,0:T(8,128)(2,1)} async-done(((bf16[128,2048]{1,0:T(8,128)(2,1)}), bf16[1024,2048]{1,0:T(8,128)(2,1)}) %all-gather.5.cloned.1.call-update) | async-done | bytes 4194320 | tf_op jit(solution)/shard_map/all_gather | solution.py:9
  96.2 5.2 %fusion.3 = f32[1024,512]{1,0:T(8,128)S(1)} fusion(bf16[1024,2048]{1,0:T(8,128)(2,1)} %all-gather.5.cloned.1.call-done, bf16[2048,512]{1,0:T(8,128)(2,1)} %all-gather.7.cloned.1.call-done), kind=kOutput, calls=%fused_computation.10 | convolution fusion | flops 2147483648 | bytes 8388608 | tf_op jit(solution)/shard_map/dot_general | solution.py:13
  101.4 42.1 %all-gather.9.cloned.1.call-done = bf16[1024,2048]{1,0:T(8,128)(2,1)} async-done(((bf16[128,2048]{1,0:T(8,128)(2,1)}), bf16[1024,2048]{1,0:T(8,128)(2,1)}) %all-gather.9.cloned.1.call-update) | async-done | bytes 4194320 | tf_op jit(solution)/shard_map/all_gather | solution.py:10
  143.6 5.9 %convolution_convert_fusion.1 = bf16[512,2048]{0,1:T(8,128)(2,1)} fusion(bf16[1024,2048]{1,0:T(8,128)(2,1)} %all-gather.9.cloned.1.call-done, f32[1024,512]{1,0:T(8,128)S(1)} %fusion.3), kind=kOutput, calls=%fused_computation.1 | convolution fusion | flops 2150105088 | bytes 8388608 | tf_op jit(solution)/shard_map/dot_general | solution.py:38
  149.5 0.0 reduce-scatter.8.cloned.1.call-update
  149.5 0.0 reduce-scatter.6.cloned.1.call-start
  149.5 29.6 %all-gather.11.cloned.1.call-done = bf16[512,2048]{1,0:T(8,128)(2,1)} async-done(((bf16[512,512]{1,0:T(8,128)(2,1)}), bf16[512,2048]{1,0:T(8,128)(2,1)}) %all-gather.11.cloned.1.call-update) | async-done | bytes 2097168 | tf_op jit(solution)/shard_map/all_gather | solution.py:19
  179.1 5.4 %multiply_convert_fusion.1 = bf16[1024,512]{1,0:T(8,128)(2,1)S(1)} fusion(f32[1024,512]{1,0:T(8,128)S(1)} %fusion.3, bf16[1024,2048]{1,0:T(8,128)(2,1)} %all-gather.9.cloned.1.call-done, bf16[512,2048]{1,0:T(8,128)(2,1)} %all-gather.11.cloned.1.call-done), kind=kOutput, calls=%fused_computation.5 | convolution fusion | flops 2149580800 | bytes 9437184 | tf_op jit(solution)/shard_map/dot_general | solution.py:17
  184.5 0.0 copy-done
  184.5 3.7 %fusion = bf16[2048,512]{0,1:T(8,128)(2,1)} fusion(bf16[1024,512]{1,0:T(8,128)(2,1)S(1)} %multiply_convert_fusion.1, bf16[1024,2048]{1,0:T(8,128)(2,1)S(1)} %copy-done), kind=kOutput, calls=%fused_computation.3 | convolution fusion | flops 2148532224 | bytes 7340032 | tf_op jit(solution)/shard_map/dot_general | solution.py:29
  188.2 0.0 reduce-scatter.6.cloned.1.call-update
  188.2 0.0 reduce-scatter.4.cloned.1.call-start
  188.3 1.6 copy-done.1
  189.9 4.3 %convolution_convert_fusion = bf16[1024,2048]{1,0:T(8,128)(2,1)} fusion(bf16[1024,512]{1,0:T(8,128)(2,1)S(1)} %multiply_convert_fusion.1, bf16[2048,512]{1,0:T(8,128)(2,1)S(1)} %copy-done.1), kind=kOutput, calls=%fused_computation | convolution fusion | flops 2149580800 | bytes 7340032 | tf_op jit(solution)/shard_map/dot_general | solution.py:48
  194.2 0.0 reduce-scatter.4.cloned.1.call-update
  194.2 23.0 %reduce-scatter.8.cloned.1.call-done = bf16[512,512]{0,1:T(8,128)(2,1)} async-done(((bf16[512,2048]{0,1:T(8,128)(2,1)}), bf16[512,512]{0,1:T(8,128)(2,1)}) %reduce-scatter.8.cloned.1.call-update) | async-done | bytes 524304 | tf_op jit(solution)/shard_map/reduce_scatter | solution.py:42
  217.1 1.2 convert_multiply_fusion
  218.3 1.3 copy.9
  219.6 35.5 %reduce-scatter.6.cloned.1.call-done = bf16[512,512]{0,1:T(8,128)(2,1)} async-done(((bf16[2048,512]{0,1:T(8,128)(2,1)}), bf16[512,512]{0,1:T(8,128)(2,1)}) %reduce-scatter.6.cloned.1.call-update) | async-done | bytes 524304 | tf_op jit(solution)/shard_map/reduce_scatter | solution.py:28
  255.2 1.2 convert_multiply_fusion.1
  256.4 1.3 copy.8
  257.7 50.3 %reduce-scatter.4.cloned.1.call-done = bf16[128,2048]{1,0:T(8,128)(2,1)} async-done(((bf16[1024,2048]{1,0:T(8,128)(2,1)}), bf16[128,2048]{1,0:T(8,128)(2,1)}) %reduce-scatter.4.cloned.1.call-update) | async-done | bytes 524304 | tf_op jit(solution)/shard_map/reduce_scatter | solution.py:52
  (2 shorter events, 0.0 us)
Async XLA Ops:
  7.2 40.6 %all-gather.7.cloned.1.call-start = ((), (), s32[]{:S(2)}) async-start(), calls=%async_computation.4 | async-start | bytes 2621440 | tf_op jit(solution)/shard_map/all_gather | solution.py:12
  7.9 88.3 %all-gather.5.cloned.1.call-start = ((), (), s32[]{:S(2)}) async-start(), calls=%async_computation.3 | async-start | bytes 4718592 | tf_op jit(solution)/shard_map/all_gather | solution.py:9
  8.6 134.9 %all-gather.9.cloned.1.call-start = ((), (), s32[]{:S(2)}) async-start(), calls=%async_computation.5 | async-start | bytes 4718592 | tf_op jit(solution)/shard_map/all_gather | solution.py:10
  9.4 169.7 %all-gather.11.cloned.1.call-start = ((), (), s32[]{:S(2)}) async-start(), calls=%async_computation.6 | async-start | bytes 2621440 | tf_op jit(solution)/shard_map/all_gather | solution.py:19
  10.0 207.2 %reduce-scatter.8.cloned.1.call-start = ((), (), s32[]{:S(2)}) async-start(), calls=%async_computation.9 | async-start | bytes 2621440 | tf_op jit(solution)/shard_map/reduce_scatter | solution.py:42
  149.5 105.7 %reduce-scatter.6.cloned.1.call-start = ((), (), s32[]{:S(2)}) async-start(), calls=%async_computation.8 | async-start | bytes 2621440 | tf_op jit(solution)/shard_map/reduce_scatter | solution.py:28
  179.1 5.4 %copy-start = (bf16[1024,2048]{1,0:T(8,128)(2,1)S(1)}, bf16[1024,2048]{1,0:T(8,128)(2,1)}, u32[]{:S(2)}) copy-start(bf16[1024,2048]{1,0:T(8,128)(2,1)} %all-gather.5.cloned.1.call-done) | copy-start | bytes 12582916
  188.2 1.6 copy-start.1
  188.2 119.7 %reduce-scatter.4.cloned.1.call-start = ((), (), s32[]{:S(2)}) async-start(), calls=%async_computation.7 | async-start | bytes 4718592 | tf_op jit(solution)/shard_map/reduce_scatter | solution.py:52
Sparse Core Ops, SparseCore 0:
  9.8 37.8 all-gather.6
  49.3 46.8 all-gather.4
  97.8 45.6 all-gather.8
  145.2 33.8 all-gather.10
  181.9 35.1 reduce-scatter.7
  220.0 35.1 reduce-scatter.5
  258.0 49.8 reduce-scatter.3
where the time goes:
time: 315 us
  waiting for transfers between devices  269 us (85%)
  matrix products  24.5 us (8%)
  between operations  14.2 us (5%)
  local copies, waits for them, and re-layouts  4.18 us (1%)
    reduce_scatter x1, waiting for transfers between devices, shards(): lax.psum_scatter(rounded.astype(jnp.float32).astype(jnp.bfloat16), 'tp',...  50.3 us
    all_gather x1, waiting for transfers between devices, shards(): lax.all_gather(tokens, 'tp', axis=0, tiled=True)  48.5 us
    all_gather x1, waiting for transfers between devices, shards(): lax.all_gather(cotangent, 'tp', axis=0, tiled=True)  42.1 us
    all_gather x1, waiting for transfers between devices, shards(): up_whole = lax.all_gather(up_weight, 'fs', axis=0, tiled=True)  37.7 us
    reduce_scatter x1, waiting for transfers between devices, shards(): lax.psum_scatter(lax.dot_general(part, dpre, (((0,), (0,)), ((), ())), pr...  35.5 us
    all_gather x1, waiting for transfers between devices, shards(): lax.all_gather(down_weight, 'fs', axis=1, tiled=True)  29.6 us
    reduce_scatter x1, waiting for transfers between devices, shards(): lax.psum_scatter(down_term.astype(jnp.bfloat16), 'fs', scatter_dimension=...  23 us
  transfers between devices with their start and end apart: 7, of which 7 were waited for; matrix products, arithmetic and copies ran while one was open for 9% of the time, Pallas kernels for 0%

commit v1 on v0

--- a/solution.py
+++ b/solution.py
@@ -9,7 +9,12 @@
         lax.all_gather(tokens, "tp", axis=0, tiled=True),
         lax.all_gather(cotangent, "tp", axis=0, tiled=True),
     )
-    up_whole = lax.all_gather(up_weight, "fs", axis=0, tiled=True)
+    ring = [up_weight]
+    for hop in range(3):
+        ring.append(lax.ppermute(ring[-1], "fs", [(dev, (dev + 1) % 4) for dev in range(4)]))
+    up_whole = jnp.roll(
+        jnp.concatenate(ring[::-1], axis=0), (lax.axis_index("fs") + 1) * ring[0].shape[0], axis=0
+    )
     pre = jnp.dot(rows_all, up_whole, preferred_element_type=jnp.float32)
     active = jnp.maximum(pre, 0.0)
     hidden = (active * active).astype(jnp.bfloat16)

time: 315 us -> 285 us (0.905)
  waiting for transfers between devices: 269 us -> 228 us
  local copies, waits for them, and re-layouts: 4.18 us -> 9.33 us
  starting transfers between devices: 0.27 us -> 4.22 us
    all_gather x1, waiting for transfers between devices: 48.5 us -> 0.01 us  [shards(): lax.all_gather(tokens, 'tp', axis=0, tiled=True)]
    ppermute x0 -> x3, waiting for transfers between devices: none -> 39.7 us  [shards(): lax.ppermute(ring[-1], 'fs', [(dev, (dev + 1) % 4) for dev in range(4)])]
    all_gather x1 -> x0, waiting for transfers between devices: 37.7 us -> none  [shards(): up_whole = lax.all_gather(up_weight, 'fs', axis=0, tiled=True)]
    reduce_scatter x1, waiting for transfers between devices: 35.5 us -> 21.9 us  [shards(): lax.psum_scatter(lax.dot_general(part, dpre, (((0,), (0,)), ((), ())), pr...]
    reduce_scatter x1, waiting for transfers between devices: 23 us -> 35.6 us  [shards(): lax.psum_scatter(down_term.astype(jnp.bfloat16), 'fs', scatter_dimension=...]
    all_gather x1, waiting for transfers between devices: 42.1 us -> 48.5 us  [shards(): lax.all_gather(cotangent, 'tp', axis=0, tiled=True)]
    unnamed x6 -> x13, local copies, waits for them, and re-layouts: 4.18 us -> 8.5 us
    ppermute x0 -> x3, starting transfers between devices: none -> 3.81 us  [shards(): lax.ppermute(ring[-1], 'fs', [(dev, (dev + 1) % 4) for dev in range(4)])]
  transfers between devices with their start and end apart: 7 -> 9, of which waited for: 7 -> 8; matrix products, arithmetic and copies ran while one was open for 9% -> 10% of each run, Pallas kernels for 0% -> 0%
where the time goes in v1:
time: 285 us; the launch traced here: 284 us
  waiting for transfers between devices  228 us (80%)
  matrix products  26.2 us (9%)
  between operations  14.2 us (5%)
  local copies, waits for them, and re-layouts  9.33 us (3%)
  starting transfers between devices  4.22 us (1%)
    reduce_scatter x1, waiting for transfers between devices, shards(): lax.psum_scatter(rounded.astype(jnp.float32).astype(jnp.bfloat16), 'tp',...  50.2 us
    all_gather x1, waiting for transfers between devices, shards(): lax.all_gather(cotangent, 'tp', axis=0, tiled=True)  48.5 us
    ppermute x3, waiting for transfers between devices, shards(): lax.ppermute(ring[-1], 'fs', [(dev, (dev + 1) % 4) for dev in range(4)])  39.7 us
    reduce_scatter x1, waiting for transfers between devices, shards(): lax.psum_scatter(down_term.astype(jnp.bfloat16), 'fs', scatter_dimension=...  35.6 us
    all_gather x1, waiting for transfers between devices, shards(): lax.all_gather(down_weight, 'fs', axis=1, tiled=True)  30 us
    reduce_scatter x1, waiting for transfers between devices, shards(): lax.psum_scatter(lax.dot_general(part, dpre, (((0,), (0,)), ((), ())), pr...  21.9 us
    unnamed x13, local copies, waits for them, and re-layouts  8.5 us
    dot_general x1, matrix products, shards(): lax.dot_general(part, up_whole, (((1,), (1,)), ((), ())), preferred_eleme...  5.94 us
  transfers between devices with their start and end apart: 9, of which 8 were waited for; matrix products, arithmetic and copies ran while one was open for 10% of the time, Pallas kernels for 0%

profile of v1, /device:TPU:0, one launch (start us, length us, event | category | flops | bytes accessed | tf_op | source)
XLA Modules:
  0.0 284.2 jit_solution(1944741191144420966)
XLA Ops:
  7.2 0.7 all-gather.4.cloned.1.call-update
  8.0 0.7 all-gather.8.cloned.1.call-update
  8.7 0.7 all-gather.6.cloned.1.call-update
  9.4 3.0 %collective-permute-start = (bf16[512,512]{1,0:T(8,128)(2,1)}, bf16[512,512]{1,0:T(8,128)(2,1)S(1)}, u32[]{:S(2)}, u32[]{:S(2)}) collective-permute-start(bf16[512,512]{1,0:T(8,128)(2,1)} %param.5), channel_id=1, source_target_pairs={{0,8},{8,16},{16,24},{24,0},{1,9},{9,17},{17,25},{25,1},{2,10},{10... | collective-permute-start | bytes 1572872 | tf_op jit(solution)/shard_map/ppermute | solution.py:14
  12.5 13.1 %collective-permute-done = bf16[512,512]{1,0:T(8,128)(2,1)S(1)} collective-permute-done((bf16[512,512]{1,0:T(8,128)(2,1)}, bf16[512,512]{1,0:T(8,128)(2,1)S(1)}, u32[]{:S(2)}, u32[]{:S(2)}) %collective-permute-start) | collective-permute-done | bytes 524320 | tf_op jit(solution)/shard_map/ppermute | solution.py:14
  25.5 0.8 collective-permute-start.1
  26.3 13.3 %collective-permute-done.1 = bf16[512,512]{1,0:T(8,128)(2,1)S(1)} collective-permute-done((bf16[512,512]{1,0:T(8,128)(2,1)S(1)}, bf16[512,512]{1,0:T(8,128)(2,1)S(1)}, u32[]{:S(2)}, u32[]{:S(2)}) %collective-permute-start.1) | collective-permute-done | bytes 524320 | tf_op jit(solution)/shard_map/ppermute | solution.py:14
  39.6 13.3 %collective-permute-done.2 = bf16[512,512]{1,0:T(8,128)(2,1)S(1)} collective-permute-done((bf16[512,512]{1,0:T(8,128)(2,1)S(1)}, bf16[512,512]{1,0:T(8,128)(2,1)S(1)}, u32[]{:S(2)}, u32[]{:S(2)}) %collective-permute-start.2) | collective-permute-done | bytes 524320 | tf_op jit(solution)/shard_map/ppermute | solution.py:14
  53.0 0.9 constant_dynamic-update-slice_fusion.7
  53.8 0.9 constant_dynamic-update-slice_fusion.6
  54.7 0.8 constant_dynamic-update-slice_fusion.5
  55.5 0.8 constant_dynamic-update-slice_fusion.4
  56.4 0.8 constant_dynamic-update-slice_fusion.3
  57.2 0.8 constant_dynamic-update-slice_fusion.2
  58.0 0.8 constant_dynamic-update-slice_fusion.1
  58.9 0.8 constant_dynamic-update-slice_fusion
  59.7 5.2 %fusion.3 = f32[512,1024]{1,0:T(8,128)S(1)} fusion(bf16[1024,2048]{1,0:T(8,128)(2,1)} %all-gather.4.cloned.1.call-done, bf16[4096,512]{1,0:T(8,128)(2,1)} %constant_dynamic-update-slice_fusion, s32[]{:T(128)S(6)} %select_n.14), kind=kOutput, calls=%fused_computation.8 | convolution fusion | flops 2147483648 | bytes 8388612 | tf_op jit(solution)/shard_map/dot_general | solution.py:18
  64.9 30.0 %all-gather.8.cloned.1.call-done = bf16[512,2048]{1,0:T(8,128)(2,1)} async-done(((bf16[512,512]{1,0:T(8,128)(2,1)}), bf16[512,2048]{1,0:T(8,128)(2,1)}) %all-gather.8.cloned.1.call-update) | async-done | bytes 2097168 | tf_op jit(solution)/shard_map/all_gather | solution.py:24
  94.9 48.5 %all-gather.6.cloned.1.call-done = bf16[1024,2048]{1,0:T(8,128)(2,1)} async-done(((bf16[128,2048]{1,0:T(8,128)(2,1)}), bf16[1024,2048]{1,0:T(8,128)(2,1)}) %all-gather.6.cloned.1.call-update) | async-done | bytes 4194320 | tf_op jit(solution)/shard_map/all_gather | solution.py:10
  143.4 5.4 %fusion.1 = bf16[1024,512]{0,1:T(8,128)(2,1)S(1)} fusion(f32[512,1024]{1,0:T(8,128)S(1)} %fusion.3, bf16[1024,2048]{1,0:T(8,128)(2,1)} %all-gather.6.cloned.1.call-done, bf16[512,2048]{1,0:T(8,128)(2,1)} %all-gather.8.cloned.1.call-done), kind=kOutput, calls=%fused_computation.5 | convolution fusion | flops 2149580800 | bytes 9437184 | tf_op jit(solution)/shard_map/dot_general | solution.py:22
  148.8 3.7 %fusion = bf16[2048,512]{0,1:T(8,128)(2,1)} fusion(bf16[1024,512]{0,1:T(8,128)(2,1)S(1)} %fusion.1, bf16[1024,2048]{1,0:T(8,128)(2,1)S(1)} %copy-done.1), kind=kOutput, calls=%fused_computation.3 | convolution fusion | flops 2148532224 | bytes 7340032 | tf_op jit(solution)/shard_map/dot_general | solution.py:34
  152.6 0.0 reduce-scatter.8.cloned.1.call-start
  152.6 5.9 %convolution_convert_fusion.1 = bf16[512,2048]{0,1:T(8,128)(2,1)} fusion(bf16[1024,2048]{1,0:T(8,128)(2,1)} %all-gather.6.cloned.1.call-done, f32[512,1024]{1,0:T(8,128)S(1)} %fusion.3), kind=kOutput, calls=%fused_computation.1 | convolution fusion | flops 2150105088 | bytes 8388608 | tf_op jit(solution)/shard_map/dot_general | solution.py:43
  158.5 0.2 reduce-scatter.4.cloned.1.call-start
  158.8 5.9 %convolution_convert_fusion = bf16[1024,2048]{1,0:T(8,128)(2,1)} fusion(bf16[1024,512]{0,1:T(8,128)(2,1)S(1)} %fusion.1, bf16[4096,512]{1,0:T(8,128)(2,1)} %constant_dynamic-update-slice_fusion, s32[]{:T(128)S(6)} %select_n.14), kind=kOutput, calls=%fused_computation | convolution fusion | flops 2149580800 | bytes 7340036 | tf_op jit(solution)/shard_map/dot_general | solution.py:53
  164.7 21.9 %reduce-scatter.6.cloned.1.call-done = bf16[512,512]{0,1:T(8,128)(2,1)} async-done(((bf16[2048,512]{0,1:T(8,128)(2,1)}), bf16[512,512]{0,1:T(8,128)(2,1)}) %reduce-scatter.6.cloned.1.call-update) | async-done | bytes 524304 | tf_op jit(solution)/shard_map/reduce_scatter | solution.py:33
  186.7 1.2 convert_multiply_fusion.1
  187.9 1.3 copy.9
  189.2 35.6 %reduce-scatter.8.cloned.1.call-done = bf16[512,512]{0,1:T(8,128)(2,1)} async-done(((bf16[512,2048]{0,1:T(8,128)(2,1)}), bf16[512,512]{0,1:T(8,128)(2,1)}) %reduce-scatter.8.cloned.1.call-update) | async-done | bytes 524304 | tf_op jit(solution)/shard_map/reduce_scatter | solution.py:47
  224.7 1.2 convert_multiply_fusion
  225.9 1.3 copy.10
  227.2 50.2 %reduce-scatter.4.cloned.1.call-done = bf16[128,2048]{1,0:T(8,128)(2,1)} async-done(((bf16[1024,2048]{1,0:T(8,128)(2,1)}), bf16[128,2048]{1,0:T(8,128)(2,1)}) %reduce-scatter.4.cloned.1.call-update) | async-done | bytes 524304 | tf_op jit(solution)/shard_map/reduce_scatter | solution.py:57
  (13 shorter events, 0.2 us)
Async XLA Ops:
  7.2 48.4 %copy-start = (bf16[512,512]{1,0:T(8,128)(2,1)S(1)}, bf16[512,512]{1,0:T(8,128)(2,1)}, u32[]{:S(2)}) copy-start(bf16[512,512]{1,0:T(8,128)(2,1)} %param.5) | copy-start | bytes 1572868
  7.2 52.5 %all-gather.4.cloned.1.call-start = ((), (), s32[]{:S(2)}) async-start(), calls=%async_computation.3 | async-start | bytes 4718592 | tf_op jit(solution)/shard_map/all_gather | solution.py:9
  7.9 87.0 %all-gather.8.cloned.1.call-start = ((), (), s32[]{:S(2)}) async-start(), calls=%async_computation.5 | async-start | bytes 2621440 | tf_op jit(solution)/shard_map/all_gather | solution.py:24
  8.7 134.8 %all-gather.6.cloned.1.call-start = ((), (), s32[]{:S(2)}) async-start(), calls=%async_computation.4 | async-start | bytes 4718592 | tf_op jit(solution)/shard_map/all_gather | solution.py:10
  9.4 177.3 %reduce-scatter.6.cloned.1.call-start = ((), (), s32[]{:S(2)}) async-start(), calls=%async_computation.7 | async-start | bytes 2621440 | tf_op jit(solution)/shard_map/reduce_scatter | solution.py:33
  9.4 16.1 %collective-permute-start = (bf16[512,512]{1,0:T(8,128)(2,1)}, bf16[512,512]{1,0:T(8,128)(2,1)S(1)}, u32[]{:S(2)}, u32[]{:S(2)}) collective-permute-start(bf16[512,512]{1,0:T(8,128)(2,1)} %param.5), channel_id=1, source_target_pairs={{0,8},{8,16},{16,24},{24,0},{1,9},{9,17},{17,25},{25,1},{2,10},{10... | collective-permute-start | bytes 1572872 | tf_op jit(solution)/shard_map/ppermute | solution.py:14
  25.5 14.1 %collective-permute-start.1 = (bf16[512,512]{1,0:T(8,128)(2,1)S(1)}, bf16[512,512]{1,0:T(8,128)(2,1)S(1)}, u32[]{:S(2)}, u32[]{:S(2)}) collective-permute-start(bf16[512,512]{1,0:T(8,128)(2,1)S(1)} %collective-permute-done), channel_id=1, source_target_pairs={{0,8},{8,16},{16,24},{24,0},{1,9},{9,17},{17,25},{25,1},{2,10},{10... | collective-permute-start | bytes 1572872 | tf_op jit(solution)/shard_map/ppermute | solution.py:14
  39.6 13.3 %collective-permute-start.2 = (bf16[512,512]{1,0:T(8,128)(2,1)S(1)}, bf16[512,512]{1,0:T(8,128)(2,1)S(1)}, u32[]{:S(2)}, u32[]{:S(2)}) collective-permute-start(bf16[512,512]{1,0:T(8,128)(2,1)S(1)} %collective-permute-done.1), channel_id=1, source_target_pairs={{0,8},{8,16},{16,24},{24,0},{1,9},{9,17},{17,25},{25,1},{2,10},{10... | collective-permute-start | bytes 1572872 | tf_op jit(solution)/shard_map/ppermute | solution.py:14
  143.4 5.4 %copy-start.1 = (bf16[1024,2048]{1,0:T(8,128)(2,1)S(1)}, bf16[1024,2048]{1,0:T(8,128)(2,1)}, u32[]{:S(2)}) copy-start(bf16[1024,2048]{1,0:T(8,128)(2,1)} %all-gather.4.cloned.1.call-done) | copy-start | bytes 12582916
  152.6 72.2 %reduce-scatter.8.cloned.1.call-start = ((), (), s32[]{:S(2)}) async-start(), calls=%async_computation.8 | async-start | bytes 2621440 | tf_op jit(solution)/shard_map/reduce_scatter | solution.py:47
  158.5 118.9 %reduce-scatter.4.cloned.1.call-start = ((), (), s32[]{:S(2)}) async-start(), calls=%async_computation.6 | async-start | bytes 4718592 | tf_op jit(solution)/shard_map/reduce_scatter | solution.py:57
Sparse Core Ops, SparseCore 0:
  9.6 49.5 all-gather.3
  61.0 33.8 all-gather.7
  96.5 46.8 all-gather.5
  152.7 33.9 reduce-scatter.5
  189.5 35.1 reduce-scatter.7
  227.5 49.8 reduce-scatter.3
